TPU v7x, 32 devices: a whole 2x2x4 slice. The times are simulated.
32 devices in a mesh: rep: 2 (over x), fs: 8 (over z, y), tp: 2 (over core).
Axes of the slice: x: 2, y: 2, z: 4, core: 2. Of those that a mesh axis runs over, the one named last changes fastest.
Arguments:
- tokens: bfloat16 [4096, 2048], P(('rep', 'fs', 'tp')), may hold values from -6 to 6
- mix_gain: float32 [2048], replicated, may hold values from 0.1 to 1.9
- conv_in_weight: bfloat16 [2048, 1024], P('fs', 'tp'), may hold values from -0.125 to 0.125
- gate_outer_weight: bfloat16 [2048, 1024], P('fs', 'tp'), may hold values from -0.125 to 0.125
- gate_inner_weight: bfloat16 [2048, 1024], P('fs', 'tp'), may hold values from -0.125 to 0.125
- conv_taps: float32 [3, 1024], P(None, 'tp'), may hold values from -3.5 to 3.5
- out_weight: bfloat16 [1024, 2048], P('tp', 'fs'), may hold values from -0.1875 to 0.1875
- ff_gain: float32 [2048], replicated, may hold values from 0.1 to 1.9
- up_weight: bfloat16 [2048, 8192], P('fs', 'tp'), may hold values from -0.125 to 0.125
- down_weight: bfloat16 [8192, 2048], P('tp', 'fs'), may hold values from -0.0625 to 0.0625
Outputs:
- layer_out: bfloat16 [4096, 2048], P(('rep', 'fs', 'tp'))
All inputs are finite; a program needn't handle non-finite values.
Results may differ from a plain program's by a relative error of at most 0.023.
Values may be sent and summed in bfloat16 or wider, within the bound.
A program may use at most 128 MiB of HBM per device.

v0:
```python
import jax
import jax.numpy as jnp
from jax import lax
from jax.sharding import PartitionSpec as P

eps = 1e-06


def rms_scale(values, gain):
    widened = values.astype(jnp.float32)
    inverse = lax.rsqrt(jnp.mean(widened * widened, axis=-1, keepdims=True) + eps)
    return (widened * inverse * gain).astype(jnp.bfloat16)


def on_device(
    tokens,
    mix_gain,
    conv_in_weight,
    gate_outer_weight,
    gate_inner_weight,
    conv_taps,
    out_weight,
    ff_gain,
    up_weight,
    down_weight,
):
    normed = rms_scale(tokens, mix_gain)
    gathered = lax.all_gather(normed, "tp", axis=0, tiled=True)
    seq_rows = gathered.shape[0]
    segment = (
        lax.all_gather(conv_in_weight, "fs", axis=0, tiled=True),
        lax.all_gather(gate_outer_weight, "fs", axis=0, tiled=True),
        lax.all_gather(gate_inner_weight, "fs", axis=0, tiled=True),
    )
    conv_input, gate_outer, gate_inner = tuple(
        (jnp.dot(gathered, weight, preferred_element_type=jnp.float32) for weight in segment)
    )
    conv_input = conv_input.astype(jnp.bfloat16)
    gate_outer = gate_outer.astype(jnp.bfloat16)
    gate_inner = gate_inner.astype(jnp.bfloat16)
    gated = gate_inner.astype(jnp.float32) * conv_input.astype(jnp.float32)
    padded = jnp.pad(gated, ((2, 0), (0, 0)))
    convolved = (
        conv_taps[0] * padded[0:seq_rows]
        + conv_taps[1] * padded[1 : seq_rows + 1]
        + conv_taps[2] * padded[2 : seq_rows + 2]
    )
    mixed = (gate_outer.astype(jnp.float32) * convolved).astype(jnp.bfloat16)
    out_full = lax.all_gather(out_weight, "fs", axis=1, tiled=True)
    lefts = mixed
    mix_total = lax.psum_scatter(
        jnp.dot(lefts, out_full, preferred_element_type=jnp.float32).astype(jnp.bfloat16),
        "tp",
        scatter_dimension=0,
        tiled=True,
    ).astype(jnp.float32)
    resid = (tokens.astype(jnp.float32) + mix_total).astype(jnp.bfloat16)
    normed_ff = rms_scale(resid, ff_gain)
    ff_gathered = lax.all_gather(normed_ff, "tp", axis=0, tiled=True)
    up_full = lax.all_gather(up_weight, "fs", axis=0, tiled=True)
    preact = jnp.dot(ff_gathered, up_full, preferred_element_type=jnp.float32)
    hidden = jnp.square(jax.nn.relu(preact)).astype(jnp.bfloat16)
    down_full = lax.all_gather(down_weight, "fs", axis=1, tiled=True)
    lefts = hidden
    ff_total = lax.psum_scatter(
        jnp.dot(lefts, down_full, preferred_element_type=jnp.float32).astype(jnp.bfloat16),
        "tp",
        scatter_dimension=0,
        tiled=True,
    ).astype(jnp.float32)
    return (resid.astype(jnp.float32) + ff_total).astype(jnp.bfloat16)


def solution(mesh):
    in_specs = (
        P(("rep", "fs", "tp"), None),
        P(),
        P("fs", "tp"),
        P("fs", "tp"),
        P("fs", "tp"),
        P(None, "tp"),
        P("tp", "fs"),
        P(),
        P("fs", "tp"),
        P("tp", "fs"),
    )
    out_specs = P(("rep", "fs", "tp"), None)
    return jax.shard_map(
        on_device, mesh=mesh, in_specs=in_specs, out_specs=out_specs, check_vma=False
    )
```

profile of v0, /device:TPU:0, one launch (start us, length us, event | category | flops | bytes accessed | tf_op | source)
XLA Modules:
  0.0 740.0 jit_solution(13610082769893983982)
XLA Ops:
  6.5 1.2 fusion.8
  7.8 2.0 fusion.10
  9.9 0.7 all-gather.15.cloned.1.call-update
  10.6 0.7 all-gather.13.cloned.1.call-update
  12.0 0.5 all-gather.17.cloned.1.call-update
  12.6 9.2 %all-gather.9.cloned.1.call-done = bf16[256,2048]{1,0:T(8,128)(2,1)} async-done(((bf16[128,2048]{1,0:T(8,128)(2,1)}), bf16[256,2048]{1,0:T(8,128)(2,1)}) %all-gather.9.cloned.1.call-update) | async-done | bytes 1048592 | tf_op jit(solution)/shard_map/all_gather | solution.py:28
  21.7 52.4 %all-gather.15.cloned.1.call-done = bf16[2048,512]{1,0:T(8,128)(2,1)} async-done(((bf16[256,512]{1,0:T(8,128)(2,1)}), bf16[2048,512]{1,0:T(8,128)(2,1)}) %all-gather.15.cloned.1.call-update) | async-done | bytes 2097168 | tf_op jit(solution)/shard_map/all_gather | solution.py:31
  74.2 2.6 fusion.7
  76.8 47.2 %all-gather.13.cloned.1.call-done = bf16[2048,512]{1,0:T(8,128)(2,1)} async-done(((bf16[256,512]{1,0:T(8,128)(2,1)}), bf16[2048,512]{1,0:T(8,128)(2,1)}) %all-gather.13.cloned.1.call-update) | async-done | bytes 2097168 | tf_op jit(solution)/shard_map/all_gather | solution.py:33
  124.0 2.3 fusion.6
  126.3 47.3 %all-gather.11.cloned.1.call-done = bf16[2048,512]{1,0:T(8,128)(2,1)} async-done(((bf16[256,512]{1,0:T(8,128)(2,1)}), bf16[2048,512]{1,0:T(8,128)(2,1)}) %all-gather.11.cloned.1.call-update) | async-done | bytes 2097168 | tf_op jit(solution)/shard_map/all_gather | solution.py:32
  173.6 50.8 %all-gather.17.cloned.1.call-done = bf16[512,2048]{1,0:T(8,128)(2,1)} async-done(((bf16[512,256]{1,0:T(8,128)(2,1)}), bf16[512,2048]{1,0:T(8,128)(2,1)}) %all-gather.17.cloned.1.call-update) | async-done | bytes 2097168 | tf_op jit(solution)/shard_map/all_gather | solution.py:49
  224.4 4.7 convolution_convert_fusion.1
  229.2 6.7 reduce-scatter.3.cloned.1.call-done
  235.9 1.3 fusion.12
  237.2 2.0 fusion.14
  239.3 0.7 all-gather.21.cloned.1.call-update
  240.0 0.7 all-gather.23.cloned.1.call-update
  240.8 8.9 %all-gather.19.cloned.1.call-done = bf16[256,2048]{1,0:T(8,128)(2,1)} async-done(((bf16[128,2048]{1,0:T(8,128)(2,1)}), bf16[256,2048]{1,0:T(8,128)(2,1)}) %all-gather.19.cloned.1.call-update) | async-done | bytes 1048592 | tf_op jit(solution)/shard_map/all_gather | solution.py:59
  249.6 230.6 %all-gather.21.cloned.1.call-done = bf16[2048,4096]{1,0:T(8,128)(2,1)} async-done(((bf16[256,4096]{1,0:T(8,128)(2,1)}), bf16[2048,4096]{1,0:T(8,128)(2,1)}) %all-gather.21.cloned.1.call-update) | async-done | bytes 16777232 | tf_op jit(solution)/shard_map/all_gather | solution.py:60
  480.2 227.6 %all-gather.23.cloned.1.call-done = bf16[4096,2048]{1,0:T(8,128)(2,1)} async-done(((bf16[4096,256]{1,0:T(8,128)(2,1)}), bf16[4096,2048]{1,0:T(8,128)(2,1)}) %all-gather.23.cloned.1.call-update) | async-done | bytes 16777232 | tf_op jit(solution)/shard_map/all_gather | solution.py:63
  707.8 16.5 %convolution_convert_fusion = bf16[256,2048]{1,0:T(8,128)(2,1)} fusion(bf16[4096,2048]{1,0:T(8,128)(2,1)} %all-gather.23.cloned.1.call-done, bf16[256,2048]{1,0:T(8,128)(2,1)} %all-gather.19.cloned.1.call-done, bf16[2048,4096]{1,0:T(8,128)(2,1)} %all-gather.21.cloned.1.call-done), kind=kOutput, calls=%fused_computation.3 | convolution fusion | flops 8593604608 | bytes 35651584 | tf_op jit(solution)/shard_map/dot_general | solution.py:66
  724.4 6.7 reduce-scatter.5.cloned.1.call-done
  731.1 2.1 fusion.15
  (28 shorter events, 1.0 us)
Async XLA Ops:
  6.5 6.0 copy-start.4
  6.5 15.2 %all-gather.9.cloned.1.call-start = ((), (), s32[]{:S(2)}) async-start(), calls=%async_computation.2 | async-start | bytes 1572864 | tf_op jit(solution)/shard_map/all_gather | solution.py:28
  9.8 64.3 %all-gather.15.cloned.1.call-start = ((), (), s32[]{:S(2)}) async-start(), calls=%async_computation.5 | async-start | bytes 2359296 | tf_op jit(solution)/shard_map/all_gather | solution.py:31
  10.6 113.4 %all-gather.13.cloned.1.call-start = ((), (), s32[]{:S(2)}) async-start(), calls=%async_computation.4 | async-start | bytes 2359296 | tf_op jit(solution)/shard_map/all_gather | solution.py:33
  11.3 162.3 %all-gather.11.cloned.1.call-start = ((), (), s32[]{:S(2)}) async-start(), calls=%async_computation.3 | async-start | bytes 2359296 | tf_op jit(solution)/shard_map/all_gather | solution.py:32
  11.9 212.5 %all-gather.17.cloned.1.call-start = ((), (), s32[]{:S(2)}) async-start(), calls=%async_computation.6 | async-start | bytes 2359296 | tf_op jit(solution)/shard_map/all_gather | solution.py:49
  12.5 223.4 %reduce-scatter.3.cloned.1.call-start = ((), (), s32[]{:S(2)}) async-start(), calls=%async_computation.7 | async-start | bytes 1572864 | tf_op jit(solution)/shard_map/reduce_scatter | solution.py:51
  21.7 102.2 %copy-start.2 = (bf16[256,2048]{1,0:T(8,128)(2,1)S(1)}, bf16[256,2048]{1,0:T(8,128)(2,1)}, u32[]{:S(2)}) copy-start(bf16[256,2048]{1,0:T(8,128)(2,1)} %all-gather.9.cloned.1.call-done) | copy-start | bytes 3145732
  224.4 11.5 %copy-start = (bf16[128,2048]{1,0:T(8,128)(2,1)S(1)}, bf16[128,2048]{1,0:T(8,128)(2,1)}, u32[]{:S(2)}) copy-start(bf16[128,2048]{1,0:T(8,128)(2,1)} %param.10) | copy-start | bytes 1572868
  229.1 8.1 %copy-start.3 = (f32[2048]{0:T(1024)S(1)}, f32[2048]{0:T(1024)}, u32[]{:S(2)}) copy-start(f32[2048]{0:T(1024)} %param.17) | copy-start | bytes 24580
  229.1 20.5 %all-gather.19.cloned.1.call-start = ((), (), s32[]{:S(2)}) async-start(), calls=%async_computation.8 | async-start | bytes 1572864 | tf_op jit(solution)/shard_map/all_gather | solution.py:59
  239.2 241.0 %all-gather.21.cloned.1.call-start = ((), (), s32[]{:S(2)}) async-start(), calls=%async_computation.9 | async-start | bytes 18874368 | tf_op jit(solution)/shard_map/all_gather | solution.py:60
  240.0 467.8 %all-gather.23.cloned.1.call-start = ((), (), s32[]{:S(2)}) async-start(), calls=%async_computation.10 | async-start | bytes 18874368 | tf_op jit(solution)/shard_map/all_gather | solution.py:63
  240.7 490.4 %copy-start.1 = (bf16[128,2048]{1,0:T(8,128)(2,1)S(1)}, bf16[128,2048]{1,0:T(8,128)(2,1)}, u32[]{:S(2)}) copy-start(bf16[128,2048]{1,0:T(8,128)(2,1)} %reduce-scatter.3.cloned.1.call-done) | copy-start | bytes 1572868
  240.7 490.4 %reduce-scatter.5.cloned.1.call-start = ((), (), s32[]{:S(2)}) async-start(), calls=%async_computation.11 | async-start | bytes 1572864 | tf_op jit(solution)/shard_map/reduce_scatter | solution.py:65
Sparse Core Ops, SparseCore 0:
  10.0 11.7 all-gather.8
  23.9 50.2 all-gather.14
  76.3 47.6 all-gather.12
  125.9 47.6 all-gather.10
  175.5 48.8 all-gather.16
  229.2 6.5 reduce-scatter.2
  239.3 10.2 all-gather.18
  251.7 228.4 all-gather.20
  482.3 225.4 all-gather.22
  724.5 6.5 reduce-scatter.4
where the time goes:
time: 740 us
  waiting for transfers between devices  691 us (93%)
  matrix products  26.2 us (4%)
  between operations  13.6 us (2%)
  other arithmetic  8.69 us (1%)
    all_gather x1, waiting for transfers between devices, on_device(): up_full = lax.all_gather(up_weight, 'fs', axis=0, tiled=True)  231 us
    all_gather x1, waiting for transfers between devices, on_device(): down_full = lax.all_gather(down_weight, 'fs', axis=1, tiled=True)  228 us
    all_gather x1, waiting for transfers between devices, on_device(): lax.all_gather(conv_in_weight, 'fs', axis=0, tiled=True)  52.4 us
    all_gather x1, waiting for transfers between devices, on_device(): out_full = lax.all_gather(out_weight, 'fs', axis=1, tiled=True)  50.8 us
    all_gather x1, waiting for transfers between devices, on_device(): lax.all_gather(gate_outer_weight, 'fs', axis=0, tiled=True)  47.3 us
    all_gather x1, waiting for transfers between devices, on_device(): lax.all_gather(gate_inner_weight, 'fs', axis=0, tiled=True)  47.2 us
    dot_general x1, matrix products, on_device(): jnp.dot(lefts, down_full, preferred_element_type=jnp.float32)  16.5 us
  transfers between devices with their start and end apart: 10, of which 10 were waited for; matrix products, arithmetic and copies ran while one was open for 1% of the time, Pallas kernels for 0%

commit v1 on v0

--- a/solution.py
+++ b/solution.py
@@ -1,9 +1,28 @@
+import functools
 import jax
 import jax.numpy as jnp
 from jax import lax
 from jax.sharding import PartitionSpec as P
 
 eps = 1e-06
+
+
+def close_table(vector, axis_key):
+    n_blocks = lax.axis_size(axis_key)
+    finding = range(n_blocks)
+    part_now = map(lambda j0: (j0, (j0 + 1) % n_blocks), finding)
+    pile = list(part_now)
+    y = [None] * n_blocks
+    y[n_blocks - 1] = vector
+    for i in range(n_blocks - 2, -1, -1):
+        y[i] = lax.ppermute(y[i + 1], axis_key, pile)
+    p_next = jnp.concatenate(y, 1)
+    extra = (lax.axis_index(axis_key) + 1) * vector.shape[1]
+    x_next = jnp.roll(p_next, extra, 1)
+    return x_next
+
+
+pieces_all_prepare = functools.partial(close_table, axis_key="fs")
 
 
 def rms_scale(values, gain):
@@ -60,7 +79,7 @@
     up_full = lax.all_gather(up_weight, "fs", axis=0, tiled=True)
     preact = jnp.dot(ff_gathered, up_full, preferred_element_type=jnp.float32)
     hidden = jnp.square(jax.nn.relu(preact)).astype(jnp.bfloat16)
-    down_full = lax.all_gather(down_weight, "fs", axis=1, tiled=True)
+    down_full = pieces_all_prepare(down_weight)
     lefts = hidden
     ff_total = lax.psum_scatter(
         jnp.dot(lefts, down_full, preferred_element_type=jnp.float32).astype(jnp.bfloat16),

time: 740 us -> 842 us (1.14)
  waiting for transfers between devices: 691 us -> 748 us
  local copies, waits for them, and re-layouts: 0.03 us -> 41.2 us
    ppermute x0 -> x7, waiting for transfers between devices: none -> 527 us  [close_table(): y[i] = lax.ppermute(y[i + 1], axis_key, pile)]
    all_gather x1, waiting for transfers between devices: 231 us -> 0.01 us  [on_device(): up_full = lax.all_gather(up_weight, 'fs', axis=0, tiled=True)]
    all_gather x1 -> x0, waiting for transfers between devices: 228 us -> none  [on_device(): down_full = lax.all_gather(down_weight, 'fs', axis=1, tiled=True)]
    unnamed x10 -> x43, local copies, waits for them, and re-layouts: 0.02 us -> 38.9 us
    all_gather x1, waiting for transfers between devices: 8.85 us -> 0.01 us  [on_device(): ff_gathered = lax.all_gather(normed_ff, 'tp', axis=0, tiled=True)]
  transfers between devices with their start and end apart: 10 -> 16, of which waited for: 10 -> 14; matrix products, arithmetic and copies ran while one was open for 1% -> 5% of each run, Pallas kernels for 0% -> 0%
where the time goes in v1:
time: 842 us; the launch traced here: 841 us
  waiting for transfers between devices  748 us (89%)
  local copies, waits for them, and re-layouts  41.2 us (5%)
  matrix products  27.6 us (3%)
  between operations  13.3 us (2%)
  other arithmetic  8.84 us (1%)
    ppermute x7, waiting for transfers between devices, close_table(): y[i] = lax.ppermute(y[i + 1], axis_key, pile)  527 us
    all_gather x1, waiting for transfers between devices, on_device(): lax.all_gather(conv_in_weight, 'fs', axis=0, tiled=True)  52.4 us
    all_gather x1, waiting for transfers between devices, on_device(): out_full = lax.all_gather(out_weight, 'fs', axis=1, tiled=True)  50.8 us
    all_gather x1, waiting for transfers between devices, on_device(): lax.all_gather(gate_outer_weight, 'fs', axis=0, tiled=True)  46.9 us
    all_gather x1, waiting for transfers between devices, on_device(): lax.all_gather(gate_inner_weight, 'fs', axis=0, tiled=True)  46.4 us
    unnamed x43, local copies, waits for them, and re-layouts  38.9 us
  transfers between devices with their start and end apart: 16, of which 14 were waited for; matrix products, arithmetic and copies ran while one was open for 5% of the time, Pallas kernels for 0%

profile of v1, /device:TPU:0, one launch (start us, length us, event | category | flops | bytes accessed | tf_op | source)
XLA Modules:
  0.0 841.3 jit_solution(695198513787674951)
XLA Ops:
  13.5 8.4 all-gather.8.cloned.1.call-done
  21.9 52.4 %all-gather.14.cloned.1.call-done = bf16[2048,512]{1,0:T(8,128)(2,1)} async-done(((bf16[256,512]{1,0:T(8,128)(2,1)}), bf16[2048,512]{1,0:T(8,128)(2,1)}) %all-gather.14.cloned.1.call-update) | async-done | bytes 2097168 | tf_op jit(solution)/shard_map/all_gather | solution.py:50
  74.3 3.4 fusion.12
  77.7 46.4 %all-gather.12.cloned.1.call-done = bf16[2048,512]{1,0:T(8,128)(2,1)} async-done(((bf16[256,512]{1,0:T(8,128)(2,1)}), bf16[2048,512]{1,0:T(8,128)(2,1)}) %all-gather.12.cloned.1.call-update) | async-done | bytes 2097168 | tf_op jit(solution)/shard_map/all_gather | solution.py:52
  124.1 2.7 fusion.11
  126.8 46.9 %all-gather.10.cloned.1.call-done = bf16[2048,512]{1,0:T(8,128)(2,1)} async-done(((bf16[256,512]{1,0:T(8,128)(2,1)}), bf16[2048,512]{1,0:T(8,128)(2,1)}) %all-gather.10.cloned.1.call-update) | async-done | bytes 2097168 | tf_op jit(solution)/shard_map/all_gather | solution.py:51
  173.7 50.8 %all-gather.16.cloned.1.call-done = bf16[512,2048]{1,0:T(8,128)(2,1)} async-done(((bf16[512,256]{1,0:T(8,128)(2,1)}), bf16[512,2048]{1,0:T(8,128)(2,1)}) %all-gather.16.cloned.1.call-update) | async-done | bytes 2097168 | tf_op jit(solution)/shard_map/all_gather | solution.py:68
  224.5 5.0 convolution_convert_fusion
  229.6 6.7 reduce-scatter.3.cloned.1.call-done
  242.3 71.6 %collective-permute-done = bf16[4096,256]{1,0:T(8,128)(2,1)S(1)} collective-permute-done((bf16[4096,256]{1,0:T(8,128)(2,1)S(1)}, bf16[4096,256]{1,0:T(8,128)(2,1)S(1)}, u32[]{:S(2)}, u32[]{:S(2)}) %collective-permute-start) | collective-permute-done | bytes 2097184 | tf_op jit(solution)/shard_map/ppermute | solution.py:18
  315.2 88.4 %collective-permute-done.1 = bf16[4096,256]{1,0:T(8,128)(2,1)S(1)} collective-permute-done((bf16[4096,256]{1,0:T(8,128)(2,1)S(1)}, bf16[4096,256]{1,0:T(8,128)(2,1)S(1)}, u32[]{:S(2)}, u32[]{:S(2)}) %collective-permute-start.1) | collective-permute-done | bytes 2097184 | tf_op jit(solution)/shard_map/ppermute | solution.py:18
  405.0 95.6 %collective-permute-done.2 = bf16[4096,256]{1,0:T(8,128)(2,1)S(1)} collective-permute-done((bf16[4096,256]{1,0:T(8,128)(2,1)S(1)}, bf16[4096,256]{1,0:T(8,128)(2,1)S(1)}, u32[]{:S(2)}, u32[]{:S(2)}) %collective-permute-start.2) | collective-permute-done | bytes 2097184 | tf_op jit(solution)/shard_map/ppermute | solution.py:18
  501.9 95.3 %collective-permute-done.3 = bf16[4096,256]{1,0:T(8,128)(2,1)S(1)} collective-permute-done((bf16[4096,256]{1,0:T(8,128)(2,1)S(1)}, bf16[4096,256]{1,0:T(8,128)(2,1)S(1)}, u32[]{:S(2)}, u32[]{:S(2)}) %collective-permute-start.3) | collective-permute-done | bytes 2097184 | tf_op jit(solution)/shard_map/ppermute | solution.py:18
  598.5 76.4 %collective-permute-done.4 = bf16[4096,256]{1,0:T(8,128)(2,1)S(1)} collective-permute-done((bf16[4096,256]{1,0:T(8,128)(2,1)S(1)}, bf16[4096,256]{1,0:T(8,128)(2,1)S(1)}, u32[]{:S(2)}, u32[]{:S(2)}) %collective-permute-start.4) | collective-permute-done | bytes 2097184 | tf_op jit(solution)/shard_map/ppermute | solution.py:18
  676.3 50.5 %collective-permute-done.5 = bf16[4096,256]{1,0:T(8,128)(2,1)} collective-permute-done((bf16[4096,256]{1,0:T(8,128)(2,1)S(1)}, bf16[4096,256]{1,0:T(8,128)(2,1)}, u32[]{:S(2)}, u32[]{:S(2)}) %collective-permute-start.5) | collective-permute-done | bytes 2097184 | tf_op jit(solution)/shard_map/ppermute | solution.py:18
  726.8 49.2 %collective-permute-done.6 = bf16[4096,256]{1,0:T(8,128)(2,1)} collective-permute-done((bf16[4096,256]{1,0:T(8,128)(2,1)}, bf16[4096,256]{1,0:T(8,128)(2,1)}, u32[]{:S(2)}, u32[]{:S(2)}) %collective-permute-start.6) | collective-permute-done | bytes 2097184 | tf_op jit(solution)/shard_map/ppermute | solution.py:18
  776.0 3.1 constant_dynamic-update-slice_fusion.15
  779.0 3.1 constant_dynamic-update-slice_fusion.14
  782.1 3.2 constant_dynamic-update-slice_fusion.13
  785.3 3.2 constant_dynamic-update-slice_fusion.12
  794.6 3.1 constant_dynamic-update-slice_fusion.7
  797.7 3.1 constant_dynamic-update-slice_fusion.6
  809.7 16.5 %fusion.4 = bf16[256,2048]{1,0:T(8,128)(2,1)} fusion(bf16[4096,4096]{1,0:T(8,128)(2,1)} %constant_dynamic-update-slice_fusion, s32[]{:T(128)S(6)} %select_n.14, bf16[256,2048]{1,0:T(8,128)(2,1)} %all-gather.18.cloned.1.call-done, bf16[2048,4096]{1,0:T(8,128)(2,1)} %all-gather.20.cloned.1.call-done), kind=kOutput, calls=%fused_computation.6 | convolution fusion | flops 8593604608 | bytes 35651588 | tf_op jit(solution)/shard_map/dot_general | solution.py:85
  826.3 6.4 reduce-scatter.5.cloned.1.call-done
  (73 shorter events, 36.6 us)
Async XLA Ops:
  6.5 229.7 %copy-start = (bf16[128,2048]{1,0:T(8,128)(2,1)S(1)}, bf16[128,2048]{1,0:T(8,128)(2,1)}, u32[]{:S(2)}) copy-start(bf16[128,2048]{1,0:T(8,128)(2,1)} %param.10) | copy-start | bytes 1572868
  6.5 231.0 %copy-start.13 = (f32[2048]{0:T(1024)S(1)}, f32[2048]{0:T(1024)}, u32[]{:S(2)}) copy-start(f32[2048]{0:T(1024)} %param.17) | copy-start | bytes 24580
  6.5 233.9 %copy-start.1 = (bf16[4096,256]{1,0:T(8,128)(2,1)S(1)}, bf16[4096,256]{1,0:T(8,128)(2,1)}, u32[]{:S(2)}) copy-start(bf16[4096,256]{1,0:T(8,128)(2,1)} %param.19) | copy-start | bytes 6291460
  6.5 15.3 %all-gather.8.cloned.1.call-start = ((), (), s32[]{:S(2)}) async-start(), calls=%async_computation.2 | async-start | bytes 1572864 | tf_op jit(solution)/shard_map/all_gather | solution.py:47
  10.0 64.3 %all-gather.14.cloned.1.call-start = ((), (), s32[]{:S(2)}) async-start(), calls=%async_computation.5 | async-start | bytes 2359296 | tf_op jit(solution)/shard_map/all_gather | solution.py:50
  10.7 113.4 %all-gather.12.cloned.1.call-start = ((), (), s32[]{:S(2)}) async-start(), calls=%async_computation.4 | async-start | bytes 2359296 | tf_op jit(solution)/shard_map/all_gather | solution.py:52
  11.5 162.3 %all-gather.10.cloned.1.call-start = ((), (), s32[]{:S(2)}) async-start(), calls=%async_computation.3 | async-start | bytes 2359296 | tf_op jit(solution)/shard_map/all_gather | solution.py:51
  12.0 212.5 %all-gather.16.cloned.1.call-start = ((), (), s32[]{:S(2)}) async-start(), calls=%async_computation.6 | async-start | bytes 2359296 | tf_op jit(solution)/shard_map/all_gather | solution.py:68
  12.6 223.6 %reduce-scatter.3.cloned.1.call-start = ((), (), s32[]{:S(2)}) async-start(), calls=%async_computation.7 | async-start | bytes 1572864 | tf_op jit(solution)/shard_map/reduce_scatter | solution.py:70
  229.5 580.2 %all-gather.18.cloned.1.call-start = ((), (), s32[]{:S(2)}) async-start(), calls=%async_computation.8 | async-start | bytes 1572864 | tf_op jit(solution)/shard_map/all_gather | solution.py:78
  239.6 570.1 %all-gather.20.cloned.1.call-start = ((), (), s32[]{:S(2)}) async-start(), calls=%async_computation.9 | async-start | bytes 18874368 | tf_op jit(solution)/shard_map/all_gather | solution.py:79
  240.4 592.3 %reduce-scatter.5.cloned.1.call-start = ((), (), s32[]{:S(2)}) async-start(), calls=%async_computation.10 | async-start | bytes 1572864 | tf_op jit(solution)/shard_map/reduce_scatter | solution.py:84
  240.4 73.4 %collective-permute-start = (bf16[4096,256]{1,0:T(8,128)(2,1)S(1)}, bf16[4096,256]{1,0:T(8,128)(2,1)S(1)}, u32[]{:S(2)}, u32[]{:S(2)}) collective-permute-start(bf16[4096,256]{1,0:T(8,128)(2,1)S(1)} %copy-done.1), channel_id=1, source_target_pairs={{0,2},{2,4},{4,6},{6,8},{8,10},{10,12},{12,14},{14,0},{1,3},{3,5},... | collective-permute-start | bytes 6291464 | tf_op jit(solution)/shard_map/ppermute | solution.py:18
  315.2 88.4 %collective-permute-start.1 = (bf16[4096,256]{1,0:T(8,128)(2,1)S(1)}, bf16[4096,256]{1,0:T(8,128)(2,1)S(1)}, u32[]{:S(2)}, u32[]{:S(2)}) collective-permute-start(bf16[4096,256]{1,0:T(8,128)(2,1)S(1)} %collective-permute-done), channel_id=1, source_target_pairs={{0,2},{2,4},{4,6},{6,8},{8,10},{10,12},{12,14},{14,0},{1,3},{3,5},... | collective-permute-start | bytes 6291464 | tf_op jit(solution)/shard_map/ppermute | solution.py:18
  405.0 95.6 %collective-permute-start.2 = (bf16[4096,256]{1,0:T(8,128)(2,1)S(1)}, bf16[4096,256]{1,0:T(8,128)(2,1)S(1)}, u32[]{:S(2)}, u32[]{:S(2)}) collective-permute-start(bf16[4096,256]{1,0:T(8,128)(2,1)S(1)} %collective-permute-done.1), channel_id=1, source_target_pairs={{0,2},{2,4},{4,6},{6,8},{8,10},{10,12},{12,14},{14,0},{1,3},{3,5},... | collective-permute-start | bytes 6291464 | tf_op jit(solution)/shard_map/ppermute | solution.py:18
  501.9 95.3 %collective-permute-start.3 = (bf16[4096,256]{1,0:T(8,128)(2,1)S(1)}, bf16[4096,256]{1,0:T(8,128)(2,1)S(1)}, u32[]{:S(2)}, u32[]{:S(2)}) collective-permute-start(bf16[4096,256]{1,0:T(8,128)(2,1)S(1)} %collective-permute-done.2), channel_id=1, source_target_pairs={{0,2},{2,4},{4,6},{6,8},{8,10},{10,12},{12,14},{14,0},{1,3},{3,5},... | collective-permute-start | bytes 6291464 | tf_op jit(solution)/shard_map/ppermute | solution.py:18
  598.5 76.4 %collective-permute-start.4 = (bf16[4096,256]{1,0:T(8,128)(2,1)S(1)}, bf16[4096,256]{1,0:T(8,128)(2,1)S(1)}, u32[]{:S(2)}, u32[]{:S(2)}) collective-permute-start(bf16[4096,256]{1,0:T(8,128)(2,1)S(1)} %collective-permute-done.3), channel_id=1, source_target_pairs={{0,2},{2,4},{4,6},{6,8},{8,10},{10,12},{12,14},{14,0},{1,3},{3,5},... | collective-permute-start | bytes 6291464 | tf_op jit(solution)/shard_map/ppermute | solution.py:18
  676.3 50.5 %collective-permute-start.5 = (bf16[4096,256]{1,0:T(8,128)(2,1)S(1)}, bf16[4096,256]{1,0:T(8,128)(2,1)}, u32[]{:S(2)}, u32[]{:S(2)}) collective-permute-start(bf16[4096,256]{1,0:T(8,128)(2,1)S(1)} %collective-permute-done.4), channel_id=1, source_target_pairs={{0,2},{2,4},{4,6},{6,8},{8,10},{10,12},{12,14},{14,0},{1,3},{3,5},... | collective-permute-start | bytes 6291464 | tf_op jit(solution)/shard_map/ppermute | solution.py:18
  726.8 49.2 %collective-permute-start.6 = (bf16[4096,256]{1,0:T(8,128)(2,1)}, bf16[4096,256]{1,0:T(8,128)(2,1)}, u32[]{:S(2)}, u32[]{:S(2)}) collective-permute-start(bf16[4096,256]{1,0:T(8,128)(2,1)} %collective-permute-done.5), channel_id=1, source_target_pairs={{0,2},{2,4},{4,6},{6,8},{8,10},{10,12},{12,14},{14,0},{1,3},{3,5},... | collective-permute-start | bytes 6291464 | tf_op jit(solution)/shard_map/ppermute | solution.py:18
  726.8 61.8 %copy-start.7 = (bf16[4096,256]{1,0:T(8,128)(2,1)S(1)}, bf16[4096,256]{1,0:T(8,128)(2,1)}, u32[]{:S(2)}) copy-start(bf16[4096,256]{1,0:T(8,128)(2,1)} %copy-done.6) | copy-start | bytes 6291460
  726.8 63.3 %copy-start.5 = (bf16[4096,256]{1,0:T(8,128)(2,1)S(1)}, bf16[4096,256]{1,0:T(8,128)(2,1)}, u32[]{:S(2)}) copy-start(bf16[4096,256]{1,0:T(8,128)(2,1)} %copy-done.4) | copy-start | bytes 6291460
  726.8 64.7 %copy-start.3 = (bf16[4096,256]{1,0:T(8,128)(2,1)S(1)}, bf16[4096,256]{1,0:T(8,128)(2,1)}, u32[]{:S(2)}) copy-start(bf16[4096,256]{1,0:T(8,128)(2,1)} %copy-done.2) | copy-start | bytes 6291460
  782.1 18.7 %copy-start.11 = (bf16[4096,256]{1,0:T(8,128)(2,1)S(1)}, bf16[4096,256]{1,0:T(8,128)(2,1)}, u32[]{:S(2)}) copy-start(bf16[4096,256]{1,0:T(8,128)(2,1)} %copy-done.10) | copy-start | bytes 6291460
  809.7 22.9 %copy-start.12 = (bf16[128,2048]{1,0:T(8,128)(2,1)S(1)}, bf16[128,2048]{1,0:T(8,128)(2,1)}, u32[]{:S(2)}) copy-start(bf16[128,2048]{1,0:T(8,128)(2,1)} %reduce-scatter.3.cloned.1.call-done) | copy-start | bytes 1572868
  (6 other events, 23.6 us)
Sparse Core Ops, SparseCore 0:
  10.1 11.7 all-gather.7
  24.0 50.2 all-gather.13
  76.4 47.6 all-gather.11
  126.1 47.6 all-gather.9
  175.6 48.8 all-gather.15
  229.6 6.5 reduce-scatter.2
  239.7 10.2 all-gather.17
  252.2 364.0 all-gather.19
  826.4 6.2 reduce-scatter.4
